TPU v7x, 32 devices: a whole 2x2x4 slice. The times are simulated.
32 devices in a mesh: ep: 16 (over z, y, x), tp: 2 (over core).
Axes of the slice: x: 2, y: 2, z: 4, core: 2. Of those that a mesh axis runs over, the one named last changes fastest.
Arguments:
- tokens: bfloat16 [1024, 2048], P('ep', 'tp'), may hold values from -6 to 6
- sequence_state_real: float32 [1024, 128, 64], P('ep', 'tp'), may hold values from -4 to 4
- sequence_state_imaginary: float32 [1024, 128, 64], P('ep', 'tp'), may hold values from -4 to 4
- mixer_norm_gain: float32 [2048], replicated, may hold values from 0.1 to 1.9
- expert_norm_gain: float32 [2048], replicated, may hold values from 0.1 to 1.9
- rate: float32 [128, 64], P('tp'), may hold values from 0.1 to 4
- freq: float32 [128, 64], P('tp'), may hold values from -3 to 3
- log_group_step: float32 [128], P('tp'), may hold values from -3 to 0
- input_map_real: float32 [128, 64, 16], P('tp'), may hold values from -1 to 1
- input_map_imaginary: float32 [128, 64, 16], P('tp'), may hold values from -1 to 1
- output_map_real: float32 [128, 16, 64], P('tp'), may hold values from -0.75 to 0.75
- output_map_imaginary: float32 [128, 16, 64], P('tp'), may hold values from -0.75 to 0.75
- skip: float32 [2048], P('tp'), may hold values from -4 to 4
- mixer_value_weight: bfloat16 [2048, 2048], P('tp'), may hold values from -0.125 to 0.125
- mixer_gate_weight: bfloat16 [2048, 2048], P('tp'), may hold values from -0.125 to 0.125
- group_router_weight: bfloat16 [2048, 4], replicated, may hold values from -0.125 to 0.125
- expert_router_weight: bfloat16 [2048, 16], replicated, may hold values from -0.125 to 0.125
- dense_blend_weight: float32 [2048], replicated, may hold values from -0.125 to 0.125
- routes: int32 [1024, 2], P('ep'), may hold values from 0 to 15, all different within a row; in each aligned block of 64 rows (0 to 63, 64 to 127, ...) at most 16 rows name the same one
- expert_gate_weight: bfloat16 [16, 2048, 1024], P('ep', None, 'tp'), may hold values from -0.125 to 0.125
- expert_up_weight: bfloat16 [16, 2048, 1024], P('ep', None, 'tp'), may hold values from -0.125 to 0.125
- expert_down_weight: bfloat16 [16, 1024, 2048], P('ep', 'tp'), may hold values from -0.1875 to 0.1875
- shared_gate_weight: bfloat16 [2048, 2048], P('tp', 'ep'), may hold values from -0.125 to 0.125
- shared_up_weight: bfloat16 [2048, 2048], P('tp', 'ep'), may hold values from -0.125 to 0.125
- shared_down_weight: bfloat16 [2048, 2048], P(None, 'tp'), may hold values from -0.125 to 0.125
Outputs:
- result: bfloat16 [1024, 2048], P('ep', 'tp')
- next_re: float32 [1024, 128, 64], P('ep', 'tp')
- next_im: float32 [1024, 128, 64], P('ep', 'tp')
Inputs may be any that keep to these rules, and one draw needn't show every extreme that they name: `routes`: each row names 2 different experts. Among the rows of one device no expert is named more than 16 times, and in every draw some expert is named exactly 16 times by some device's rows.
All inputs are finite; a program needn't handle non-finite values.
Results may differ from a plain program's by a relative error of at most 0.017.
Values may be sent and summed in bfloat16 or wider, within the bound.
A program may use at most 128 MiB of HBM per device.

v0:
```python
import jax
import jax.numpy as jnp
from jax import lax
from jax.sharding import PartitionSpec as P

NG = 4
EPS = 1e-06
PRECISION_MAX = lax.Precision.HIGHEST


def state_factors(rate, freq, log_group_step, input_map_real, input_map_imaginary):
    step_size = jnp.exp(log_group_step)[:, None]
    magnitude = jnp.exp(-rate * step_size)
    abar_re = magnitude * jnp.cos(freq * step_size)
    abar_im = magnitude * jnp.sin(freq * step_size)
    denom = rate * rate + freq * freq
    shift_re = abar_re - 1.0
    fac_re = (abar_im * freq - shift_re * rate) / denom
    fac_im = -(abar_im * rate + shift_re * freq) / denom
    bbar_re = fac_re[:, :, None] * input_map_real - fac_im[:, :, None] * input_map_imaginary
    bbar_im = fac_re[:, :, None] * input_map_imaginary + fac_im[:, :, None] * input_map_real
    return (abar_re, abar_im, bbar_re, bbar_im)


def state_step(
    normed,
    sequence_state_real,
    sequence_state_imaginary,
    factors,
    output_map_real,
    output_map_imaginary,
    skip,
):
    abar_re, abar_im, bbar_re, bbar_im = factors
    groups = abar_re.shape[0]
    inputs = normed.astype(jnp.float32)
    grouped = inputs.reshape(inputs.shape[0], groups, -1)
    drive_re = jnp.einsum("tgc,gpc->tgp", grouped, bbar_re, precision=PRECISION_MAX)
    drive_im = jnp.einsum("tgc,gpc->tgp", grouped, bbar_im, precision=PRECISION_MAX)
    fresh_real = abar_re * sequence_state_real - abar_im * sequence_state_imaginary + drive_re
    fresh_imaginary = abar_re * sequence_state_imaginary + abar_im * sequence_state_real + drive_im
    state_readout = jnp.einsum("dor,zdr->zdo", output_map_real, fresh_real, precision=PRECISION_MAX)
    state_readout = state_readout - jnp.einsum(
        "dor,zdr->zdo", output_map_imaginary, fresh_imaginary, precision=PRECISION_MAX
    )
    mixed = state_readout.reshape(inputs.shape) + skip * inputs
    return (mixed, fresh_real, fresh_imaginary)


def pair_product(left, first_map, second_map):
    first = jnp.dot(left, first_map, preferred_element_type=jnp.float32)
    second = jnp.dot(left, second_map, preferred_element_type=jnp.float32)
    return jnp.concatenate([first, second], axis=1)


def shards(
    tokens,
    sequence_state_real,
    sequence_state_imaginary,
    mixer_norm_gain,
    expert_norm_gain,
    rate,
    freq,
    log_group_step,
    input_map_real,
    input_map_imaginary,
    output_map_real,
    output_map_imaginary,
    skip,
    mixer_value_weight,
    mixer_gate_weight,
    group_router_weight,
    expert_router_weight,
    dense_blend_weight,
    routes,
    expert_gate_weight,
    expert_up_weight,
    expert_down_weight,
    shared_gate_weight,
    shared_up_weight,
    shared_down_weight,
):
    seq_rows, half_width = tokens.shape
    width = 2 * half_width
    column_start = lax.axis_index("tp") * half_width

    def own_rows(values):
        return lax.dynamic_slice_in_dim(values, column_start, half_width, 0)

    float_tokens = tokens.astype(jnp.float32)
    square_sum = lax.psum(jnp.sum(float_tokens * float_tokens, axis=1), "tp")
    first_scale = lax.rsqrt(square_sum / width + EPS)[:, None]
    normed = (float_tokens * first_scale * own_rows(mixer_norm_gain)).astype(jnp.bfloat16)
    factors = state_factors(rate, freq, log_group_step, input_map_real, input_map_imaginary)
    mixed, next_re, next_im = state_step(
        normed,
        sequence_state_real,
        sequence_state_imaginary,
        factors,
        output_map_real,
        output_map_imaginary,
        skip,
    )
    activated = jax.nn.gelu(mixed).astype(jnp.bfloat16)
    value_part = jnp.dot(activated, mixer_value_weight, preferred_element_type=jnp.float32)
    gate_part = jnp.dot(activated, mixer_gate_weight, preferred_element_type=jnp.float32)
    stacked = jnp.stack([value_part, gate_part], axis=1)
    mix_sum = lax.psum_scatter(
        stacked.astype(jnp.bfloat16), "tp", scatter_dimension=2, tiled=True
    ).astype(jnp.float32)
    mix_half = (mix_sum[:, 0] * jax.nn.sigmoid(mix_sum[:, 1])).astype(jnp.bfloat16)
    hidden = (float_tokens + mix_half.astype(jnp.float32)).astype(jnp.bfloat16)
    hidden_f32 = hidden.astype(jnp.float32)
    scaled = hidden_f32 * own_rows(expert_norm_gain)
    router_map = jnp.concatenate(
        [own_rows(group_router_weight), own_rows(expert_router_weight)], axis=1
    ).astype(jnp.float32)
    blend_map = own_rows(dense_blend_weight)
    hidden_squares = jnp.sum(hidden_f32 * hidden_f32, axis=1)
    total_squares = lax.psum(hidden_squares, "tp")
    inverse = lax.rsqrt(total_squares / width + EPS)[:, None]
    normal_rows = scaled * inverse
    raw_part = jnp.dot(normal_rows, router_map, precision=PRECISION_MAX)
    blend_part = jnp.dot(normal_rows, blend_map, precision=PRECISION_MAX)
    logits, blend_logit = lax.psum((raw_part, blend_part), "tp")
    hnorm = (scaled * inverse).astype(jnp.bfloat16)
    experts = expert_router_weight.shape[1]
    top_count = routes.shape[1]
    per_group = experts // NG
    group_prob = jax.nn.softmax(logits[:, :NG], axis=-1)
    expert_logits = logits[:, NG:]
    expert_hits = routes[:, :, None] == jnp.arange(experts, dtype=jnp.int32)[None, None, :]
    chosen = jnp.sum(jnp.where(expert_hits, expert_logits[:, None, :], 0.0), axis=2)
    group_hits = (routes // per_group)[:, :, None] == jnp.arange(NG, dtype=jnp.int32)[None, None, :]
    group_sel = jnp.sum(jnp.where(group_hits, group_prob[:, None, :], 0.0), axis=2)
    weights = jax.nn.softmax(chosen, axis=1) * group_sel
    full_rows = lax.all_gather(hnorm, "tp", axis=1, tiled=True)
    capacity = max(2, 2 * seq_rows * top_count // experts)
    flat_routes = routes.reshape(-1)
    matches = (flat_routes[:, None] == jnp.arange(experts, dtype=jnp.int32)[None, :]).astype(
        jnp.int32
    )
    slot_rank = jnp.sum(jnp.cumsum(matches, axis=0) * matches, axis=1) - 1
    slot_target = flat_routes * capacity + slot_rank
    dispatch = slot_target[None, :] == jnp.arange(experts * capacity, dtype=jnp.int32)[:, None]
    dispatch_rows = jnp.sum(
        dispatch.reshape(experts * capacity, seq_rows, top_count).astype(jnp.float32), axis=2
    )
    outgoing = jnp.dot(
        dispatch_rows.astype(jnp.bfloat16), full_rows, preferred_element_type=jnp.float32
    )
    outgoing = outgoing.astype(jnp.bfloat16).reshape(experts, capacity, width)
    received = lax.all_to_all(outgoing, "ep", split_axis=0, concat_axis=0, tiled=True)
    sources = received.shape[0]
    items = received.shape[1]
    token_rows = received.reshape(sources * items, width)
    gate_e = jnp.dot(token_rows, expert_gate_weight[0], preferred_element_type=jnp.float32)
    expert_up_rows = jnp.dot(token_rows, expert_up_weight[0], preferred_element_type=jnp.float32)
    inner = (jax.nn.silu(gate_e) * expert_up_rows).astype(jnp.bfloat16)
    part_out = jnp.dot(inner, expert_down_weight[0], preferred_element_type=jnp.float32)
    total = lax.psum_scatter(part_out.astype(jnp.bfloat16), "tp", scatter_dimension=1, tiled=True)
    finished = total.reshape(sources, items, half_width)
    returned = lax.all_to_all(finished, "ep", split_axis=0, concat_axis=0, tiled=True)
    returned_flat = returned.reshape(experts * capacity, half_width)
    picked = returned_flat[slot_target].reshape(seq_rows, top_count, half_width).astype(jnp.float32)
    routed = jnp.sum(weights[:, :, None] * picked, axis=1)
    partial_dense = pair_product(
        lax.all_gather(hnorm, "ep", axis=0, tiled=True), shared_gate_weight, shared_up_weight
    )
    dense_sum = lax.psum(partial_dense.astype(jnp.bfloat16), "tp").astype(jnp.float32)
    dense_cols = shared_gate_weight.shape[1]
    inner_cols = (jax.nn.silu(dense_sum[:, :dense_cols]) * dense_sum[:, dense_cols:]).astype(
        jnp.bfloat16
    )
    dense_inner = lax.all_to_all(inner_cols, "ep", split_axis=0, concat_axis=1, tiled=True)
    dense_out = jnp.dot(dense_inner, shared_down_weight, preferred_element_type=jnp.float32)
    result = hidden_f32 + routed + jax.nn.sigmoid(blend_logit)[:, None] * dense_out
    return (result.astype(jnp.bfloat16), next_re, next_im)


def solution(mesh):
    placed = (
        P("ep", "tp"),
        P("ep", "tp", None),
        P("ep", "tp", None),
        P(),
        P(),
        P("tp", None),
        P("tp", None),
        P("tp"),
        P("tp", None, None),
        P("tp", None, None),
        P("tp", None, None),
        P("tp", None, None),
        P("tp"),
        P("tp", None),
        P("tp", None),
        P(),
        P(),
        P(),
        P("ep", None),
        P("ep", None, "tp"),
        P("ep", None, "tp"),
        P("ep", "tp", None),
        P("tp", "ep"),
        P("tp", "ep"),
        P(None, "tp"),
    )
    return jax.shard_map(
        shards,
        mesh=mesh,
        in_specs=placed,
        out_specs=(P("ep", "tp"), P("ep", "tp", None), P("ep", "tp", None)),
        check_vma=False,
    )
```

profile of v0, /device:TPU:0, one launch (start us, length us, event | category | flops | bytes accessed | tf_op | source)
XLA Modules:
  0.0 187.7 jit_solution(3510667995029894204)
XLA Ops:
  7.2 3.5 %copy.64 = f32[64,64,64]{0,2,1:T(8,128)} copy(f32[64,64,64]{2,1,0:T(8,128)} %param.27) | data formatting | bytes 2097152 | tf_op args[2]
  10.7 3.4 %copy.63 = f32[64,64,64]{0,2,1:T(8,128)} copy(f32[64,64,64]{2,1,0:T(8,128)} %param.26) | data formatting | bytes 2097152 | tf_op args[1]
  14.3 2.6 %psum.35 = f32[64]{0:T(128)S(1)} all-reduce(f32[64]{0:T(128)S(1)} %fusion.29), channel_id=1, replica_groups=mesh['ep'=16,'tp'=2] {'tp'}, use_global_device_ids=true, to_apply=%region_1.0 | all-reduce | flops 64 | bytes 512 | tf_op jit(solution)/shard_map/psum | solution.py:91
  19.8 4.9 %bitcast_add_fusion.1 = f32[64,64,64]{0,2,1:T(8,128)S(1)} fusion(f32[64,64,64]{0,2,1:T(8,128)} %copy.64, f32[64,64,64]{0,2,1:T(8,128)} %copy.63, bf16[64,64,16]{0,2,1:T(8,128)(2,1)S(1)} %bitcast.75, f32[64,64]{1,0:T(8,128)S(1)} %get-tuple-element.17, f32[64,64]{1,0:T(8,128)S(1)} %get-tuple-element.18, f32[64,64,16]{1,2,0:T(8,128)S(1)} %copy-done.7, ...), kind=kOutput, calls=%fused_computation.13 | convolution fusion | flops 51576832 | bytes 3866624 | tf_op jit(solution)/shard_map/tgc,gpc->tgp/dot_general | solution.py:38
  24.8 3.2 %bitcast_add_fusion = f32[64,64,64]{0,2,1:T(8,128)S(1)} fusion(f32[64,64,64]{0,2,1:T(8,128)S(1)} %copy-done.4, f32[64,64,64]{0,2,1:T(8,128)S(1)} %copy-done.3, bf16[64,64,16]{0,2,1:T(8,128)(2,1)S(1)} %bitcast.76, f32[64,64]{1,0:T(8,128)S(1)} %get-tuple-element.17, f32[64,64]{1,0:T(8,128)S(1)} %get-tuple-element.18, f32[64,64,16]{1,2,0:T(8,128)S(1)} %copy-done.8, ...), kind=kOutput, calls=%fused_computation.12 | convolution fusion | flops 51576832 | bytes 3866624 | tf_op jit(solution)/shard_map/tgc,gpc->tgp/dot_general | solution.py:39
  30.0 1.9 %convolution_subtract_fusion = f32[64,64,16]{1,2,0:T(8,128)S(1)} fusion(f32[64,64,16]{1,2,0:T(8,128)S(1)} %fusion.77, f32[64,64,64]{0,2,1:T(8,128)S(1)} %bitcast_add_fusion, f32[64,16,64]{2,1,0:T(8,128)S(1)} %copy-done.10), kind=kOutput, calls=%fused_computation.15 | convolution fusion | flops 50397184 | bytes 1835008 | tf_op jit(solution)/shard_map/dor,zdr->zdo/dot_general | solution.py:43
  32.1 3.3 %fusion.1 = bf16[64,1,2048]{2,0,1:T(8,128)(2,1)S(1)} fusion(bf16[1024,2048]{1,0:T(8,128)(2,1)} %param.39, f32[64,1024]{1,0:T(8,128)S(1)} %copy.70, f32[1024]{0:T(1024)S(1)} %copy-done.14, f32[1024]{0:T(1024)S(1)} %dynamic_slice.15, f32[64]{0:T(128)S(1)} %add_rsqrt_fusion.1, bf16[64,1024]{1,0:T(8,128)(2,1)S(1)} %copy-done.6), kind=kOutput, calls=%fused_computation.6 | convolution fusion | flops 269615104 | bytes 4858112 | tf_op jit(solution)/shard_map/dot_general | solution.py:106
  37.8 10.3 %reduce-scatter.3.cloned.1.call-done = bf16[64,2,1024]{2,0,1:T(8,128)(2,1)} async-done(((bf16[64,2,2048]{2,0,1:T(8,128)(2,1)}), bf16[64,2,1024]{2,0,1:T(8,128)(2,1)}) %reduce-scatter.3.cloned.1.call-update) | async-done | bytes 262160 | tf_op jit(solution)/shard_map/reduce_scatter | solution.py:108
  49.3 2.5 %psum.36 = f32[64]{0:T(128)S(1)} all-reduce(f32[64]{0:T(128)S(1)} %get-tuple-element.14), channel_id=1, replica_groups=mesh['ep'=16,'tp'=2] {'tp'}, use_global_device_ids=true, to_apply=%region_4.0 | all-reduce | flops 64 | bytes 512 | tf_op jit(solution)/shard_map/psum | solution.py:120
  53.4 2.3 %all_gather.6 = bf16[64,2048]{1,0:T(8,128)(2,1)S(1)} all-gather(bf16[64,1024]{1,0:T(8,128)(2,1)} %fusion.43), channel_id=1, replica_groups=mesh['ep'=16,'tp'=2] {'tp'}, dimensions={1}, use_global_device_ids=true | all-gather | bytes 393216 | tf_op jit(solution)/shard_map/all_gather | solution.py:137
  56.2 41.0 %all_to_all.29 = bf16[16,16,2048]{2,1,0:T(8,128)(2,1)S(1)} all-to-all(bf16[16,16,2048]{2,1,0:T(8,128)(2,1)S(1)} %bitcast.74), channel_id=1, replica_groups=mesh['ep'=16,'tp'=2] {'ep'}, dimensions={0} | all-to-all | bytes 2097152 | tf_op jit(solution)/shard_map/all_to_all | solution.py:153
  98.9 4.2 %convolution_convert_fusion = bf16[256,2048]{1,0:T(8,128)(2,1)} fusion(bf16[1,512,2048]{2,1,0:T(8,128)(2,1)S(1)} %copy-done, bf16[256,2048]{1,0:T(8,128)(2,1)} %bitcast.79, bf16[1,2048,512]{2,1,0:T(8,128)(2,1)} %param.45, f32[256,512]{1,0:T(8,128)S(1)} %fusion.5), kind=kOutput, calls=%fused_computation.1 | convolution fusion | flops 1075052544 | bytes 6815744 | tf_op jit(solution)/shard_map/dot_general | solution.py:160
  103.1 3.8 %copy.77 = f32[64,64,64]{2,1,0:T(8,128)} copy(f32[64,64,64]{0,2,1:T(8,128)} %copy-done.2) | data formatting | bytes 2097152
  106.9 3.8 %copy.78 = f32[64,64,64]{2,1,0:T(8,128)} copy(f32[64,64,64]{0,2,1:T(8,128)} %copy-done.1) | data formatting | bytes 2097152
  111.7 3.3 %all-reduce = (f32[64,20]{0,1:T(8,128)S(1)}, f32[64]{0:T(128)S(1)}) all-reduce(f32[64,20]{0,1:T(8,128)S(1)} %fusion.44, f32[64]{0:T(128)S(1)} %convolution_bitcast_fusion), channel_id=1, replica_groups=mesh['ep'=16,'tp'=2] {'tp'}, use_global_device_ids=true, to_apply=%region_5.0 | all-reduce | flops 1344 | bytes 10752 | tf_op jit(solution)/shard_map/psum | solution.py:125
  115.1 3.4 %all-gather.2.cloned.1.call-done = bf16[1024,1024]{1,0:T(8,128)(2,1)} async-done(((bf16[64,1024]{1,0:T(8,128)(2,1)}), bf16[1024,1024]{1,0:T(8,128)(2,1)}) %all-gather.2.cloned.1.call-update) | async-done | bytes 2097168 | tf_op jit(solution)/shard_map/all_gather | solution.py:168
  118.5 2.4 %convolution_convert_fusion.4 = bf16[1024,128]{0,1:T(8,128)(2,1)S(1)} fusion(bf16[1024,1024]{1,0:T(8,128)(2,1)} %all-gather.2.cloned.1.call-done, bf16[1024,128]{1,0:T(8,128)(2,1)S(1)} %copy-done.12), kind=kOutput, calls=%fused_computation.17 | convolution fusion | flops 268566528 | bytes 2621440 | tf_op jit(solution)/shard_map/dot_general | solution.py:52
  120.9 7.1 %reduce-scatter.5.cloned.1.call-done = bf16[256,1024]{1,0:T(8,128)(2,1)} async-done(((bf16[256,2048]{1,0:T(8,128)(2,1)}), bf16[256,1024]{1,0:T(8,128)(2,1)}) %reduce-scatter.5.cloned.1.call-update) | async-done | bytes 524304 | tf_op jit(solution)/shard_map/reduce_scatter | solution.py:161
  128.0 6.8 %all-to-all-start.1 = ((bf16[16,16,1024]{2,1,0:T(8,128)(2,1)}), bf16[16,16,1024]{2,1,0:T(8,128)(2,1)S(1)}, u32[]{:S(2)}, u32[]{:S(2)}) async-start(bf16[16,16,1024]{2,1,0:T(8,128)(2,1)} %bitcast.80), calls=%async_computation.3 | async-start | bytes 1048576 | tf_op jit(solution)/shard_map/all_to_all | solution.py:163
  134.9 2.4 %convolution_convert_fusion.5 = bf16[1024,128]{0,1:T(8,128)(2,1)S(1)} fusion(bf16[1024,1024]{1,0:T(8,128)(2,1)} %all-gather.2.cloned.1.call-done, bf16[1024,128]{1,0:T(8,128)(2,1)S(1)} %copy-done.13), kind=kOutput, calls=%fused_computation.18 | convolution fusion | flops 268566528 | bytes 2621440 | tf_op jit(solution)/shard_map/dot_general | solution.py:51
  138.2 20.0 %all-reduce.3.cloned.1.call-done = bf16[1024,256]{0,1:T(8,128)(2,1)} async-done(((bf16[1024,256]{0,1:T(8,128)(2,1)}), bf16[1024,256]{0,1:T(8,128)(2,1)}) %all-reduce.3.cloned.1.call-update) | async-done | bytes 524304 | tf_op jit(solution)/shard_map/psum | solution.py:170
  160.3 6.8 %all-to-all-start.2 = ((bf16[16,64,128]{2,1,0:T(8,128)(2,1)}), bf16[16,64,128]{2,1,0:T(8,128)(2,1)S(1)}, u32[]{:S(2)}, u32[]{:S(2)}) async-start(bf16[16,64,128]{2,1,0:T(8,128)(2,1)} %bitcast.19), calls=%async_computation.4 | async-start | bytes 524288 | tf_op jit(solution)/shard_map/all_to_all | solution.py:175
  169.2 8.2 %all-to-all-done.2 = bf16[16,64,128]{2,1,0:T(8,128)(2,1)S(1)} async-done(((bf16[16,64,128]{2,1,0:T(8,128)(2,1)}), bf16[16,64,128]{2,1,0:T(8,128)(2,1)S(1)}, u32[]{:S(2)}, u32[]{:S(2)}) %all-to-all-start.2) | async-done | bytes 262176 | tf_op jit(solution)/shard_map/all_to_all | solution.py:175
  177.5 3.7 %fusion.14 = bf16[64,1024]{1,0:T(8,128)(2,1)} fusion(bf16[2048,1024]{1,0:T(8,128)(2,1)} %param.49, f32[64,1024]{1,0:T(8,128)S(1)} %multiply_reduce_fusion, bf16[64,1024]{1,0:T(8,128)(2,1)S(1)} %get-tuple-element.15, f32[64]{0:T(128)S(1)} %add_divide_fusion, bf16[16,64,128]{2,1,0:T(8,128)(2,1)S(1)} %all-to-all-done.2), kind=kOutput, calls=%fused_computation.21 | convolution fusion | flops 268763136 | bytes 4980992 | tf_op jit(solution)/shard_map/dot_general | solution.py:176
  (109 shorter events, 18.4 us)
Async XLA Ops:
  7.2 91.7 %copy-start = (bf16[1,512,2048]{2,1,0:T(8,128)(2,1)S(1)}, bf16[1,512,2048]{2,1,0:T(8,128)(2,1)}, u32[]{:S(2)}) copy-start(bf16[1,512,2048]{2,1,0:T(8,128)(2,1)} %param.46) | copy-start | bytes 6291460
  7.2 40.9 %reduce-scatter.3.cloned.1.call-start = ((), (), s32[]{:S(2)}) async-start(), calls=%async_computation.5 | async-start | bytes 786432 | tf_op jit(solution)/shard_map/reduce_scatter | solution.py:108
  10.7 3.4 %copy-start.6 = (bf16[64,1024]{1,0:T(8,128)(2,1)S(1)}, bf16[64,1024]{1,0:T(8,128)(2,1)}, u32[]{:S(2)}) copy-start(bf16[64,1024]{1,0:T(8,128)(2,1)} %param.25) | copy-start | bytes 393220
  10.7 6.2 %copy-start.18 = (f32[2048]{0:T(1024)S(1)}, f32[2048]{0:T(1024)}, u32[]{:S(2)}) copy-start(f32[2048]{0:T(1024)} %param.28) | copy-start | bytes 24580
  10.7 8.0 %copy-start.21 = (f32[64]{0:T(128)S(1)}, f32[64]{0:T(128)}, u32[]{:S(2)}) copy-start(f32[64]{0:T(128)} %param.32) | copy-start | bytes 772
  10.7 9.1 %copy-start.7 = (f32[64,64,16]{1,2,0:T(8,128)S(1)}, f32[64,64,16]{1,2,0:T(8,128)}, u32[]{:S(2)}) copy-start(f32[64,64,16]{1,2,0:T(8,128)} %param.34) | copy-start | bytes 786436
  10.7 9.1 %copy-start.8 = (f32[64,64,16]{1,2,0:T(8,128)S(1)}, f32[64,64,16]{1,2,0:T(8,128)}, u32[]{:S(2)}) copy-start(f32[64,64,16]{1,2,0:T(8,128)} %param.33) | copy-start | bytes 786436
  19.8 5.0 %copy-start.3 = (f32[64,64,64]{0,2,1:T(8,128)S(1)}, f32[64,64,64]{0,2,1:T(8,128)}, u32[]{:S(2)}) copy-start(f32[64,64,64]{0,2,1:T(8,128)} %copy.64) | copy-start | bytes 3145732
  19.8 5.0 %copy-start.4 = (f32[64,64,64]{0,2,1:T(8,128)S(1)}, f32[64,64,64]{0,2,1:T(8,128)}, u32[]{:S(2)}) copy-start(f32[64,64,64]{0,2,1:T(8,128)} %copy.63) | copy-start | bytes 3145732
  24.8 3.3 %copy-start.2 = (f32[64,64,64]{0,2,1:T(8,128)}, f32[64,64,64]{0,2,1:T(8,128)S(1)}, u32[]{:S(2)}) copy-start(f32[64,64,64]{0,2,1:T(8,128)S(1)} %bitcast_add_fusion.1) | copy-start | bytes 3145732
  24.8 3.3 %copy-start.11 = (f32[64,16,64]{2,1,0:T(8,128)S(1)}, f32[64,16,64]{2,1,0:T(8,128)}, u32[]{:S(2)}) copy-start(f32[64,16,64]{2,1,0:T(8,128)} %param.35) | copy-start | bytes 786436
  28.0 3.9 %copy-start.1 = (f32[64,64,64]{0,2,1:T(8,128)}, f32[64,64,64]{0,2,1:T(8,128)S(1)}, u32[]{:S(2)}) copy-start(f32[64,64,64]{0,2,1:T(8,128)S(1)} %bitcast_add_fusion) | copy-start | bytes 3145732
  32.1 3.5 %copy-start.5 = (bf16[1024,2048]{1,0:T(8,128)(2,1)S(1)}, bf16[1024,2048]{1,0:T(8,128)(2,1)}, u32[]{:S(2)}) copy-start(bf16[1024,2048]{1,0:T(8,128)(2,1)} %param.38) | copy-start | bytes 12582916
  37.4 81.1 %all-gather.2.cloned.1.call-start = ((), (), s32[]{:S(2)}) async-start(), calls=%async_computation.7 | async-start | bytes 2228224 | tf_op jit(solution)/shard_map/all_gather | solution.py:168
  52.5 75.5 %reduce-scatter.5.cloned.1.call-start = ((), (), s32[]{:S(2)}) async-start(), calls=%async_computation.6 | async-start | bytes 1572864 | tf_op jit(solution)/shard_map/reduce_scatter | solution.py:161
  53.3 44.9 %copy-start.20 = (bf16[1,2048,512]{2,1,0:T(8,128)(2,1)S(1)}, bf16[1,2048,512]{2,1,0:T(8,128)(2,1)}, u32[]{:S(2)}) copy-start(bf16[1,2048,512]{2,1,0:T(8,128)(2,1)} %param.44) | copy-start | bytes 6291460
  106.9 4.0 %copy-start.17 = (bf16[2048,4]{0,1:T(4,128)(2,1)S(1)}, bf16[2048,4]{0,1:T(4,128)(2,1)}, u32[]{:S(2)}) copy-start(bf16[2048,4]{0,1:T(4,128)(2,1)} %param.40) | copy-start | bytes 49156
  106.9 4.0 %copy-start.15 = (bf16[2048,16]{0,1:T(8,128)(2,1)S(1)}, bf16[2048,16]{0,1:T(8,128)(2,1)}, u32[]{:S(2)}) copy-start(bf16[2048,16]{0,1:T(8,128)(2,1)} %param.41) | copy-start | bytes 196612
  106.9 4.1 %dynamic-slice-start = ((f32[2048]{0:T(1024)}, s32[]{:T(128)}), f32[1024]{0:T(1024)S(1)}, s32[]{:S(2)}) async-start(f32[2048]{0:T(1024)} %param.42, s32[]{:T(128)} %select_n.30), calls=%async_computation.9 | async-start | bytes 8704 | tf_op jit(solution)/shard_map/dynamic_slice | solution.py:88
  106.9 11.6 %copy-start.12 = (bf16[1024,128]{1,0:T(8,128)(2,1)S(1)}, bf16[1024,128]{1,0:T(8,128)(2,1)}, u32[]{:S(2)}) copy-start(bf16[1024,128]{1,0:T(8,128)(2,1)} %param.48) | copy-start | bytes 786436
  111.0 23.9 %copy-start.13 = (bf16[1024,128]{1,0:T(8,128)(2,1)S(1)}, bf16[1024,128]{1,0:T(8,128)(2,1)}, u32[]{:S(2)}) copy-start(bf16[1024,128]{1,0:T(8,128)(2,1)} %param.47) | copy-start | bytes 786436
  128.0 32.3 %all-to-all-start.1 = ((bf16[16,16,1024]{2,1,0:T(8,128)(2,1)}), bf16[16,16,1024]{2,1,0:T(8,128)(2,1)S(1)}, u32[]{:S(2)}, u32[]{:S(2)}) async-start(bf16[16,16,1024]{2,1,0:T(8,128)(2,1)} %bitcast.80), calls=%async_computation.3 | async-start | bytes 1048576 | tf_op jit(solution)/shard_map/all_to_all | solution.py:163
  134.8 23.4 %all-reduce.3.cloned.1.call-start = ((), (), s32[]{:S(2)}) async-start(), calls=%async_computation.8 | async-start | bytes 1048576 | tf_op jit(solution)/shard_map/psum | solution.py:170
  160.3 17.1 %all-to-all-start.2 = ((bf16[16,64,128]{2,1,0:T(8,128)(2,1)}), bf16[16,64,128]{2,1,0:T(8,128)(2,1)S(1)}, u32[]{:S(2)}, u32[]{:S(2)}) async-start(bf16[16,64,128]{2,1,0:T(8,128)(2,1)} %bitcast.19), calls=%async_computation.4 | async-start | bytes 524288 | tf_op jit(solution)/shard_map/all_to_all | solution.py:175
  (5 other events, 8.9 us)
Sparse Core Ops, SparseCore 0:
  37.6 10.4 reduce-scatter.2
  52.6 65.8 all-gather.1
  120.8 7.2 reduce-scatter.4
  138.3 19.8 all-reduce.2
where the time goes:
time: 188 us
  blocking collectives  51.7 us (28%)
  waiting for transfers between devices  49.1 us (26%)
  matrix products  30.9 us (16%)
  local copies, waits for them, and re-layouts  19.7 us (10%)
  between operations  14.3 us (8%)
  starting transfers between devices  13.8 us (7%)
  other arithmetic  8.23 us (4%)
    all_to_all x1, blocking collectives, shards(): lax.all_to_all(outgoing, 'ep', split_axis=0, concat_axis=0, tiled=True)  41 us
    psum x1, waiting for transfers between devices, shards(): lax.psum(partial_dense.astype(jnp.bfloat16), 'tp').astype(jnp.float32)  20 us
    unnamed x49, local copies, waits for them, and re-layouts  15.8 us
    reduce_scatter x1, waiting for transfers between devices, shards(): lax.psum_scatter(stacked.astype(jnp.bfloat16), 'tp', scatter_dimension=2,...  10.3 us
    all_to_all x1, waiting for transfers between devices, shards(): lax.all_to_all(inner_cols, 'ep', split_axis=0, concat_axis=1, tiled=True)  8.24 us
    reduce_scatter x1, waiting for transfers between devices, shards(): lax.psum_scatter(part_out.astype(jnp.bfloat16), 'tp', scatter_dimension=1...  7.08 us
    all_to_all x1, starting transfers between devices, shards(): lax.all_to_all(inner_cols, 'ep', split_axis=0, concat_axis=1, tiled=True)  6.83 us
    all_to_all x1, starting transfers between devices, shards(): lax.all_to_all(finished, 'ep', split_axis=0, concat_axis=0, tiled=True)  6.79 us
  transfers between devices with their start and end apart: 6, of which 5 were waited for; matrix products, arithmetic and copies ran while one was open for 13% of the time, Pallas kernels for 0%

commit v1 on v0

--- a/solution.py
+++ b/solution.py
@@ -150,7 +150,19 @@
         dispatch_rows.astype(jnp.bfloat16), full_rows, preferred_element_type=jnp.float32
     )
     outgoing = outgoing.astype(jnp.bfloat16).reshape(experts, capacity, width)
-    received = lax.all_to_all(outgoing, "ep", split_axis=0, concat_axis=0, tiled=True)
+    ways, here = (lax.axis_size("ep"), lax.axis_index("ep"))
+    width_2 = outgoing.shape[0] // ways
+    shape = list(outgoing.shape)
+    shape[0] = width_2
+    height = shape[0]
+    shape[0] = height * ways
+    full = jnp.zeros(shape, outgoing.dtype)
+    for mask in range(ways):
+        part = lax.dynamic_slice_in_dim(outgoing, (here ^ mask) * width_2, width_2, axis=0)
+        if mask:
+            part = lax.ppermute(part, "ep", [(d, d ^ mask) for d in range(ways)])
+        full = lax.dynamic_update_slice_in_dim(full, part, (here ^ mask) * height, axis=0)
+    received = full
     sources = received.shape[0]
     items = received.shape[1]
     token_rows = received.reshape(sources * items, width)

time: 188 us -> 223 us (1.19)
  waiting for transfers between devices: 49.1 us -> 96.6 us
  blocking collectives: 51.7 us -> 10.6 us
  starting transfers between devices: 13.8 us -> 42.7 us
    all_gather x1, waiting for transfers between devices: 3.41 us -> 56.3 us  [shards(): lax.all_gather(hnorm, 'ep', axis=0, tiled=True)]
    all_to_all x1 -> x0, blocking collectives: 41 us -> none  [shards(): lax.all_to_all(outgoing, 'ep', split_axis=0, concat_axis=0, tiled=True)]
    ppermute x0 -> x15, starting transfers between devices: none -> 31.1 us  [shards(): part = lax.ppermute(part, 'ep', [(d, d ^ mask) for d in range(ways)])]
    reduce_scatter x1, waiting for transfers between devices: 7.08 us -> 0.01 us  [shards(): lax.psum_scatter(part_out.astype(jnp.bfloat16), 'tp', scatter_dimension=1...]
    ppermute x0 -> x15, waiting for transfers between devices: none -> 4.39 us  [shards(): part = lax.ppermute(part, 'ep', [(d, d ^ mask) for d in range(ways)])]
    psum x1, waiting for transfers between devices: 20 us -> 17.5 us  [shards(): lax.psum(partial_dense.astype(jnp.bfloat16), 'tp').astype(jnp.float32)]
    unnamed x49 -> x53, local copies, waits for them, and re-layouts: 15.8 us -> 16 us
  transfers between devices with their start and end apart: 6 -> 21, of which waited for: 5 -> 6; matrix products, arithmetic and copies ran while one was open for 13% -> 8% of each run, Pallas kernels for 0% -> 0%
where the time goes in v1:
time: 223 us
  waiting for transfers between devices  96.6 us (43%)
  starting transfers between devices  42.7 us (19%)
  matrix products  30.4 us (14%)
  local copies, waits for them, and re-layouts  20.4 us (9%)
  between operations  14.6 us (7%)
  blocking collectives  10.6 us (5%)
  other arithmetic  7.56 us (3%)
    all_gather x1, waiting for transfers between devices, shards(): lax.all_gather(hnorm, 'ep', axis=0, tiled=True)  56.3 us
    ppermute x15, starting transfers between devices, shards(): part = lax.ppermute(part, 'ep', [(d, d ^ mask) for d in range(ways)])  31.1 us
    psum x1, waiting for transfers between devices, shards(): lax.psum(partial_dense.astype(jnp.bfloat16), 'tp').astype(jnp.float32)  17.5 us
    unnamed x53, local copies, waits for them, and re-layouts  16 us
    reduce_scatter x1, waiting for transfers between devices, shards(): lax.psum_scatter(stacked.astype(jnp.bfloat16), 'tp', scatter_dimension=2,...  9.45 us
    all_to_all x1, waiting for transfers between devices, shards(): lax.all_to_all(inner_cols, 'ep', split_axis=0, concat_axis=1, tiled=True)  8.24 us
    all_to_all x1, starting transfers between devices, shards(): lax.all_to_all(inner_cols, 'ep', split_axis=0, concat_axis=1, tiled=True)  6.83 us
    dot_general x1, matrix products, state_step(): jnp.einsum('tgc,gpc->tgp', grouped, bbar_re, precision=PRECISION_MAX)  4.93 us
  transfers between devices with their start and end apart: 21, of which 6 were waited for; matrix products, arithmetic and copies ran while one was open for 8% of the time, Pallas kernels for 0%

profile of v1, /device:TPU:0, one launch (start us, length us, event | category | flops | bytes accessed | tf_op | source)
XLA Modules:
  0.0 222.8 jit_solution(11777853794460047601)
XLA Ops:
  7.2 3.5 %copy.64 = f32[64,64,64]{0,2,1:T(8,128)} copy(f32[64,64,64]{2,1,0:T(8,128)} %param.27) | data formatting | bytes 2097152 | tf_op args[2]
  10.7 3.4 %copy.63 = f32[64,64,64]{0,2,1:T(8,128)} copy(f32[64,64,64]{2,1,0:T(8,128)} %param.26) | data formatting | bytes 2097152 | tf_op args[1]
  14.3 2.6 %psum.35 = f32[64]{0:T(128)S(1)} all-reduce(f32[64]{0:T(128)S(1)} %fusion.16), channel_id=1, replica_groups=mesh['ep'=16,'tp'=2] {'tp'}, use_global_device_ids=true, to_apply=%region_1.0 | all-reduce | flops 64 | bytes 512 | tf_op jit(solution)/shard_map/psum | solution.py:91
  19.8 4.9 %bitcast_add_fusion.1 = f32[64,64,64]{0,2,1:T(8,128)S(1)} fusion(f32[64,64,64]{0,2,1:T(8,128)} %copy.64, f32[64,64,64]{0,2,1:T(8,128)} %copy.63, bf16[64,64,16]{0,2,1:T(8,128)(2,1)S(1)} %bitcast.73, f32[64,64]{1,0:T(8,128)S(1)} %get-tuple-element.33, f32[64,64]{1,0:T(8,128)S(1)} %get-tuple-element.34, f32[64,64,16]{1,2,0:T(8,128)S(1)} %copy-done.8, ...), kind=kOutput, calls=%fused_computation.13 | convolution fusion | flops 51576832 | bytes 3866624 | tf_op jit(solution)/shard_map/tgc,gpc->tgp/dot_general | solution.py:38
  24.8 3.2 %bitcast_add_fusion = f32[64,64,64]{0,2,1:T(8,128)S(1)} fusion(f32[64,64,64]{0,2,1:T(8,128)S(1)} %copy-done.4, f32[64,64,64]{0,2,1:T(8,128)S(1)} %copy-done.3, bf16[64,64,16]{0,2,1:T(8,128)(2,1)S(1)} %bitcast.74, f32[64,64]{1,0:T(8,128)S(1)} %get-tuple-element.33, f32[64,64]{1,0:T(8,128)S(1)} %get-tuple-element.34, f32[64,64,16]{1,2,0:T(8,128)S(1)} %copy-done.9, ...), kind=kOutput, calls=%fused_computation.12 | convolution fusion | flops 51576832 | bytes 3866624 | tf_op jit(solution)/shard_map/tgc,gpc->tgp/dot_general | solution.py:39
  32.1 3.3 %fusion.1 = bf16[64,1,2048]{2,0,1:T(8,128)(2,1)S(1)} fusion(bf16[1024,2048]{1,0:T(8,128)(2,1)} %param.39, f32[64,1024]{1,0:T(8,128)S(1)} %copy.70, f32[1024]{0:T(1024)S(1)} %copy-done.16, f32[1024]{0:T(1024)S(1)} %dynamic_slice.63, f32[64]{0:T(128)S(1)} %add_rsqrt_fusion.1, bf16[64,1024]{1,0:T(8,128)(2,1)S(1)} %copy-done.7), kind=kOutput, calls=%fused_computation.6 | convolution fusion | flops 269615104 | bytes 4858112 | tf_op jit(solution)/shard_map/dot_general | solution.py:106
  38.6 9.5 %reduce-scatter.3.cloned.1.call-done = bf16[64,2,1024]{2,0,1:T(8,128)(2,1)} async-done(((bf16[64,2,2048]{2,0,1:T(8,128)(2,1)}), bf16[64,2,1024]{2,0,1:T(8,128)(2,1)}) %reduce-scatter.3.cloned.1.call-update) | async-done | bytes 262160 | tf_op jit(solution)/shard_map/reduce_scatter | solution.py:108
  64.3 2.7 %collective-permute-start.7 = (bf16[1,16,2048]{2,1,0:T(8,128)(2,1)S(1)}, bf16[1,16,2048]{2,1,0:T(8,128)(2,1)S(1)}, u32[]{:S(2)}, u32[]{:S(2)}) collective-permute-start(bf16[1,16,2048]{2,1,0:T(8,128)(2,1)S(1)} %get-tuple-element.23), channel_id=1, source_target_pairs={{0,16},{2,18},{4,20},{6,22},{8,24},{10,26},{12,28},{14,30},{16,0},... | collective-permute-start | bytes 196616 | tf_op jit(solution)/shard_map/ppermute | solution.py:163
  68.6 3.4 %collective-permute-start.9 = (bf16[1,16,2048]{2,1,0:T(8,128)(2,1)S(1)}, bf16[1,16,2048]{2,1,0:T(8,128)(2,1)S(1)}, u32[]{:S(2)}, u32[]{:S(2)}) collective-permute-start(bf16[1,16,2048]{2,1,0:T(8,128)(2,1)S(1)} %get-tuple-element.21), channel_id=1, source_target_pairs={{0,20},{2,22},{4,16},{6,18},{8,28},{10,30},{12,24},{14,26},{16,4},... | collective-permute-start | bytes 196616 | tf_op jit(solution)/shard_map/ppermute | solution.py:163
  72.3 3.6 %collective-permute-start.11 = (bf16[1,16,2048]{2,1,0:T(8,128)(2,1)S(1)}, bf16[1,16,2048]{2,1,0:T(8,128)(2,1)S(1)}, u32[]{:S(2)}, u32[]{:S(2)}) collective-permute-start(bf16[1,16,2048]{2,1,0:T(8,128)(2,1)S(1)} %get-tuple-element.19), channel_id=1, source_target_pairs={{0,24},{2,26},{4,28},{6,30},{8,16},{10,18},{12,20},{14,22},{16,8},... | collective-permute-start | bytes 196616 | tf_op jit(solution)/shard_map/ppermute | solution.py:163
  78.2 4.3 %collective-permute-start.13 = (bf16[1,16,2048]{2,1,0:T(8,128)(2,1)S(1)}, bf16[1,16,2048]{2,1,0:T(8,128)(2,1)S(1)}, u32[]{:S(2)}, u32[]{:S(2)}) collective-permute-start(bf16[1,16,2048]{2,1,0:T(8,128)(2,1)S(1)} %get-tuple-element.17), channel_id=1, source_target_pairs={{0,28},{2,30},{4,24},{6,26},{8,20},{10,22},{12,16},{14,18},{16,12}... | collective-permute-start | bytes 196616 | tf_op jit(solution)/shard_map/ppermute | solution.py:163
  82.6 3.6 %collective-permute-start.14 = (bf16[1,16,2048]{2,1,0:T(8,128)(2,1)S(1)}, bf16[1,16,2048]{2,1,0:T(8,128)(2,1)S(1)}, u32[]{:S(2)}, u32[]{:S(2)}) collective-permute-start(bf16[1,16,2048]{2,1,0:T(8,128)(2,1)S(1)} %get-tuple-element.16), channel_id=1, source_target_pairs={{0,30},{2,28},{4,26},{6,24},{8,22},{10,20},{12,18},{14,16},{16,14}... | collective-permute-start | bytes 196616 | tf_op jit(solution)/shard_map/ppermute | solution.py:163
  86.4 4.2 %collective-permute-done.14 = bf16[1,16,2048]{2,1,0:T(8,128)(2,1)S(1)} collective-permute-done((bf16[1,16,2048]{2,1,0:T(8,128)(2,1)S(1)}, bf16[1,16,2048]{2,1,0:T(8,128)(2,1)S(1)}, u32[]{:S(2)}, u32[]{:S(2)}) %collective-permute-start.14) | collective-permute-done | bytes 65568 | tf_op jit(solution)/shard_map/ppermute | solution.py:163
  93.1 4.4 %convolution_convert_fusion = bf16[256,2048]{1,0:T(8,128)(2,1)} fusion(bf16[1,512,2048]{2,1,0:T(8,128)(2,1)S(1)} %copy-done, f32[256,512]{1,0:T(8,128)} %fusion.3, bf16[256,2048]{1,0:T(8,128)(2,1)} %bitcast.77, bf16[1,2048,512]{2,1,0:T(8,128)(2,1)} %param.44), kind=kOutput, calls=%fused_computation.1 | convolution fusion | flops 1075052544 | bytes 6815744 | tf_op jit(solution)/shard_map/dot_general | solution.py:172
  98.2 3.8 %copy.77 = f32[64,64,64]{2,1,0:T(8,128)} copy(f32[64,64,64]{0,2,1:T(8,128)} %copy-done.2) | data formatting | bytes 2097152
  102.0 4.1 %copy.78 = f32[64,64,64]{2,1,0:T(8,128)} copy(f32[64,64,64]{0,2,1:T(8,128)} %copy-done.1) | data formatting | bytes 2097152
  107.1 3.3 %all-reduce = (f32[64,20]{0,1:T(8,128)S(1)}, f32[64]{0:T(128)S(1)}) all-reduce(f32[64,20]{0,1:T(8,128)S(1)} %fusion.31, f32[64]{0:T(128)S(1)} %convolution_bitcast_fusion), channel_id=1, replica_groups=mesh['ep'=16,'tp'=2] {'tp'}, use_global_device_ids=true, to_apply=%region_5.0 | all-reduce | flops 1344 | bytes 10752 | tf_op jit(solution)/shard_map/psum | solution.py:125
  110.5 4.6 %all-to-all-start = ((bf16[16,16,1024]{2,1,0:T(8,128)(2,1)}), bf16[16,16,1024]{2,1,0:T(8,128)(2,1)S(1)}, u32[]{:S(2)}, u32[]{:S(2)}) async-start(bf16[16,16,1024]{2,1,0:T(8,128)(2,1)} %bitcast.79), calls=%async_computation.2 | async-start | bytes 1048576 | tf_op jit(solution)/shard_map/all_to_all | solution.py:175
  115.1 56.3 %all-gather.2.cloned.1.call-done = bf16[1024,1024]{1,0:T(8,128)(2,1)} async-done(((bf16[64,1024]{1,0:T(8,128)(2,1)}), bf16[1024,1024]{1,0:T(8,128)(2,1)}) %all-gather.2.cloned.1.call-update) | async-done | bytes 2097168 | tf_op jit(solution)/shard_map/all_gather | solution.py:180
  171.5 2.6 %convolution_convert_fusion.4 = bf16[1024,128]{0,1:T(8,128)(2,1)S(1)} fusion(bf16[1024,1024]{1,0:T(8,128)(2,1)} %all-gather.2.cloned.1.call-done, bf16[1024,128]{1,0:T(8,128)(2,1)S(1)} %copy-done.14), kind=kOutput, calls=%fused_computation.15 | convolution fusion | flops 268566528 | bytes 2621440 | tf_op jit(solution)/shard_map/dot_general | solution.py:52
  175.8 17.5 %all-reduce.3.cloned.1.call-done = bf16[1024,256]{0,1:T(8,128)(2,1)} async-done(((bf16[1024,256]{0,1:T(8,128)(2,1)}), bf16[1024,256]{0,1:T(8,128)(2,1)}) %all-reduce.3.cloned.1.call-update) | async-done | bytes 524304 | tf_op jit(solution)/shard_map/psum | solution.py:182
  195.5 6.8 %all-to-all-start.1 = ((bf16[16,64,128]{2,1,0:T(8,128)(2,1)}), bf16[16,64,128]{2,1,0:T(8,128)(2,1)S(1)}, u32[]{:S(2)}, u32[]{:S(2)}) async-start(bf16[16,64,128]{2,1,0:T(8,128)(2,1)} %bitcast.78), calls=%async_computation.3 | async-start | bytes 524288 | tf_op jit(solution)/shard_map/all_to_all | solution.py:187
  204.3 8.2 %all-to-all-done.1 = bf16[16,64,128]{2,1,0:T(8,128)(2,1)S(1)} async-done(((bf16[16,64,128]{2,1,0:T(8,128)(2,1)}), bf16[16,64,128]{2,1,0:T(8,128)(2,1)S(1)}, u32[]{:S(2)}, u32[]{:S(2)}) %all-to-all-start.1) | async-done | bytes 262176 | tf_op jit(solution)/shard_map/all_to_all | solution.py:187
  212.6 3.7 %fusion.8 = bf16[64,1024]{1,0:T(8,128)(2,1)} fusion(bf16[2048,1024]{1,0:T(8,128)(2,1)} %param.49, f32[64,1024]{1,0:T(8,128)S(1)} %multiply_reduce_fusion, bf16[64,1024]{1,0:T(8,128)(2,1)S(1)} %get-tuple-element.15, f32[64]{0:T(128)S(1)} %add_divide_fusion, bf16[16,64,128]{2,1,0:T(8,128)(2,1)S(1)} %all-to-all-done.1), kind=kOutput, calls=%fused_computation.19 | convolution fusion | flops 268763136 | bytes 4980992 | tf_op jit(solution)/shard_map/dot_general | solution.py:188
  (159 shorter events, 40.8 us)
Async XLA Ops:
  7.2 86.0 %copy-start = (bf16[1,512,2048]{2,1,0:T(8,128)(2,1)S(1)}, bf16[1,512,2048]{2,1,0:T(8,128)(2,1)}, u32[]{:S(2)}) copy-start(bf16[1,512,2048]{2,1,0:T(8,128)(2,1)} %param.46) | copy-start | bytes 6291460
  7.2 40.9 %reduce-scatter.3.cloned.1.call-start = ((), (), s32[]{:S(2)}) async-start(), calls=%async_computation.4 | async-start | bytes 786432 | tf_op jit(solution)/shard_map/reduce_scatter | solution.py:108
  37.4 73.0 %reduce-scatter.5.cloned.1.call-start = ((), (), s32[]{:S(2)}) async-start(), calls=%async_computation.5 | async-start | bytes 1572864 | tf_op jit(solution)/shard_map/reduce_scatter | solution.py:173
  54.8 6.7 %collective-permute-start = (bf16[1,16,2048]{2,1,0:T(8,128)(2,1)S(1)}, bf16[1,16,2048]{2,1,0:T(8,128)(2,1)S(1)}, u32[]{:S(2)}, u32[]{:S(2)}) collective-permute-start(bf16[1,16,2048]{2,1,0:T(8,128)(2,1)S(1)} %get-tuple-element.30), channel_id=1, source_target_pairs={{0,2},{2,0},{4,6},{6,4},{8,10},{10,8},{12,14},{14,12},{16,18},{18,... | collective-permute-start | bytes 196616 | tf_op jit(solution)/shard_map/ppermute | solution.py:163
  56.6 7.4 %collective-permute-start.1 = (bf16[1,16,2048]{2,1,0:T(8,128)(2,1)S(1)}, bf16[1,16,2048]{2,1,0:T(8,128)(2,1)S(1)}, u32[]{:S(2)}, u32[]{:S(2)}) collective-permute-start(bf16[1,16,2048]{2,1,0:T(8,128)(2,1)S(1)} %get-tuple-element.29), channel_id=1, source_target_pairs={{0,4},{2,6},{4,0},{6,2},{8,12},{10,14},{12,8},{14,10},{16,20},{18,... | collective-permute-start | bytes 196616 | tf_op jit(solution)/shard_map/ppermute | solution.py:163
  58.0 6.3 %collective-permute-start.2 = (bf16[1,16,2048]{2,1,0:T(8,128)(2,1)S(1)}, bf16[1,16,2048]{2,1,0:T(8,128)(2,1)S(1)}, u32[]{:S(2)}, u32[]{:S(2)}) collective-permute-start(bf16[1,16,2048]{2,1,0:T(8,128)(2,1)S(1)} %get-tuple-element.28), channel_id=1, source_target_pairs={{0,6},{2,4},{4,2},{6,0},{8,14},{10,12},{12,10},{14,8},{16,22},{18,... | collective-permute-start | bytes 196616 | tf_op jit(solution)/shard_map/ppermute | solution.py:163
  58.4 8.7 %collective-permute-start.3 = (bf16[1,16,2048]{2,1,0:T(8,128)(2,1)S(1)}, bf16[1,16,2048]{2,1,0:T(8,128)(2,1)S(1)}, u32[]{:S(2)}, u32[]{:S(2)}) collective-permute-start(bf16[1,16,2048]{2,1,0:T(8,128)(2,1)S(1)} %get-tuple-element.27), channel_id=1, source_target_pairs={{0,8},{2,10},{4,12},{6,14},{8,0},{10,2},{12,4},{14,6},{16,24},{18,... | collective-permute-start | bytes 196616 | tf_op jit(solution)/shard_map/ppermute | solution.py:163
  60.1 8.5 %collective-permute-start.4 = (bf16[1,16,2048]{2,1,0:T(8,128)(2,1)S(1)}, bf16[1,16,2048]{2,1,0:T(8,128)(2,1)S(1)}, u32[]{:S(2)}, u32[]{:S(2)}) collective-permute-start(bf16[1,16,2048]{2,1,0:T(8,128)(2,1)S(1)} %get-tuple-element.26), channel_id=1, source_target_pairs={{0,10},{2,8},{4,14},{6,12},{8,2},{10,0},{12,6},{14,4},{16,26},{18,... | collective-permute-start | bytes 196616 | tf_op jit(solution)/shard_map/ppermute | solution.py:163
  61.5 10.4 %collective-permute-start.5 = (bf16[1,16,2048]{2,1,0:T(8,128)(2,1)S(1)}, bf16[1,16,2048]{2,1,0:T(8,128)(2,1)S(1)}, u32[]{:S(2)}, u32[]{:S(2)}) collective-permute-start(bf16[1,16,2048]{2,1,0:T(8,128)(2,1)S(1)} %get-tuple-element.25), channel_id=1, source_target_pairs={{0,12},{2,14},{4,8},{6,10},{8,4},{10,6},{12,0},{14,2},{16,28},{18,... | collective-permute-start | bytes 196616 | tf_op jit(solution)/shard_map/ppermute | solution.py:163
  63.9 8.4 %collective-permute-start.6 = (bf16[1,16,2048]{2,1,0:T(8,128)(2,1)S(1)}, bf16[1,16,2048]{2,1,0:T(8,128)(2,1)S(1)}, u32[]{:S(2)}, u32[]{:S(2)}) collective-permute-start(bf16[1,16,2048]{2,1,0:T(8,128)(2,1)S(1)} %get-tuple-element.24), channel_id=1, source_target_pairs={{0,14},{2,12},{4,10},{6,8},{8,6},{10,4},{12,2},{14,0},{16,30},{18,... | collective-permute-start | bytes 196616 | tf_op jit(solution)/shard_map/ppermute | solution.py:163
  64.3 11.6 %collective-permute-start.7 = (bf16[1,16,2048]{2,1,0:T(8,128)(2,1)S(1)}, bf16[1,16,2048]{2,1,0:T(8,128)(2,1)S(1)}, u32[]{:S(2)}, u32[]{:S(2)}) collective-permute-start(bf16[1,16,2048]{2,1,0:T(8,128)(2,1)S(1)} %get-tuple-element.23), channel_id=1, source_target_pairs={{0,16},{2,18},{4,20},{6,22},{8,24},{10,26},{12,28},{14,30},{16,0},... | collective-permute-start | bytes 196616 | tf_op jit(solution)/shard_map/ppermute | solution.py:163
  67.0 11.2 %collective-permute-start.8 = (bf16[1,16,2048]{2,1,0:T(8,128)(2,1)S(1)}, bf16[1,16,2048]{2,1,0:T(8,128)(2,1)S(1)}, u32[]{:S(2)}, u32[]{:S(2)}) collective-permute-start(bf16[1,16,2048]{2,1,0:T(8,128)(2,1)S(1)} %get-tuple-element.22), channel_id=1, source_target_pairs={{0,18},{2,16},{4,22},{6,20},{8,26},{10,24},{12,30},{14,28},{16,2},... | collective-permute-start | bytes 196616 | tf_op jit(solution)/shard_map/ppermute | solution.py:163
  68.6 14.0 %collective-permute-start.9 = (bf16[1,16,2048]{2,1,0:T(8,128)(2,1)S(1)}, bf16[1,16,2048]{2,1,0:T(8,128)(2,1)S(1)}, u32[]{:S(2)}, u32[]{:S(2)}) collective-permute-start(bf16[1,16,2048]{2,1,0:T(8,128)(2,1)S(1)} %get-tuple-element.21), channel_id=1, source_target_pairs={{0,20},{2,22},{4,16},{6,18},{8,28},{10,30},{12,24},{14,26},{16,4},... | collective-permute-start | bytes 196616 | tf_op jit(solution)/shard_map/ppermute | solution.py:163
  72.0 14.4 %collective-permute-start.10 = (bf16[1,16,2048]{2,1,0:T(8,128)(2,1)S(1)}, bf16[1,16,2048]{2,1,0:T(8,128)(2,1)S(1)}, u32[]{:S(2)}, u32[]{:S(2)}) collective-permute-start(bf16[1,16,2048]{2,1,0:T(8,128)(2,1)S(1)} %get-tuple-element.20), channel_id=1, source_target_pairs={{0,22},{2,20},{4,18},{6,16},{8,30},{10,28},{12,26},{14,24},{16,6},... | collective-permute-start | bytes 196616 | tf_op jit(solution)/shard_map/ppermute | solution.py:163
  72.3 14.0 %collective-permute-start.11 = (bf16[1,16,2048]{2,1,0:T(8,128)(2,1)S(1)}, bf16[1,16,2048]{2,1,0:T(8,128)(2,1)S(1)}, u32[]{:S(2)}, u32[]{:S(2)}) collective-permute-start(bf16[1,16,2048]{2,1,0:T(8,128)(2,1)S(1)} %get-tuple-element.19), channel_id=1, source_target_pairs={{0,24},{2,26},{4,28},{6,30},{8,16},{10,18},{12,20},{14,22},{16,8},... | collective-permute-start | bytes 196616 | tf_op jit(solution)/shard_map/ppermute | solution.py:163
  76.0 10.4 %collective-permute-start.12 = (bf16[1,16,2048]{2,1,0:T(8,128)(2,1)S(1)}, bf16[1,16,2048]{2,1,0:T(8,128)(2,1)S(1)}, u32[]{:S(2)}, u32[]{:S(2)}) collective-permute-start(bf16[1,16,2048]{2,1,0:T(8,128)(2,1)S(1)} %get-tuple-element.18), channel_id=1, source_target_pairs={{0,26},{2,24},{4,30},{6,28},{8,18},{10,16},{12,22},{14,20},{16,10}... | collective-permute-start | bytes 196616 | tf_op jit(solution)/shard_map/ppermute | solution.py:163
  78.2 8.2 %collective-permute-start.13 = (bf16[1,16,2048]{2,1,0:T(8,128)(2,1)S(1)}, bf16[1,16,2048]{2,1,0:T(8,128)(2,1)S(1)}, u32[]{:S(2)}, u32[]{:S(2)}) collective-permute-start(bf16[1,16,2048]{2,1,0:T(8,128)(2,1)S(1)} %get-tuple-element.17), channel_id=1, source_target_pairs={{0,28},{2,30},{4,24},{6,26},{8,20},{10,22},{12,16},{14,18},{16,12}... | collective-permute-start | bytes 196616 | tf_op jit(solution)/shard_map/ppermute | solution.py:163
  82.6 8.0 %collective-permute-start.14 = (bf16[1,16,2048]{2,1,0:T(8,128)(2,1)S(1)}, bf16[1,16,2048]{2,1,0:T(8,128)(2,1)S(1)}, u32[]{:S(2)}, u32[]{:S(2)}) collective-permute-start(bf16[1,16,2048]{2,1,0:T(8,128)(2,1)S(1)} %get-tuple-element.16), channel_id=1, source_target_pairs={{0,30},{2,28},{4,26},{6,24},{8,22},{10,20},{12,18},{14,16},{16,14}... | collective-permute-start | bytes 196616 | tf_op jit(solution)/shard_map/ppermute | solution.py:163
  97.5 74.0 %all-gather.2.cloned.1.call-start = ((), (), s32[]{:S(2)}) async-start(), calls=%async_computation.6 | async-start | bytes 2228224 | tf_op jit(solution)/shard_map/all_gather | solution.py:180
  102.0 69.4 %copy-start.14 = (bf16[1024,128]{1,0:T(8,128)(2,1)S(1)}, bf16[1024,128]{1,0:T(8,128)(2,1)}, u32[]{:S(2)}) copy-start(bf16[1024,128]{1,0:T(8,128)(2,1)} %param.48) | copy-start | bytes 786436
  106.3 67.7 %copy-start.15 = (bf16[1024,128]{1,0:T(8,128)(2,1)S(1)}, bf16[1024,128]{1,0:T(8,128)(2,1)}, u32[]{:S(2)}) copy-start(bf16[1024,128]{1,0:T(8,128)(2,1)} %param.47) | copy-start | bytes 786436
  110.5 85.0 %all-to-all-start = ((bf16[16,16,1024]{2,1,0:T(8,128)(2,1)}), bf16[16,16,1024]{2,1,0:T(8,128)(2,1)S(1)}, u32[]{:S(2)}, u32[]{:S(2)}) async-start(bf16[16,16,1024]{2,1,0:T(8,128)(2,1)} %bitcast.79), calls=%async_computation.2 | async-start | bytes 1048576 | tf_op jit(solution)/shard_map/all_to_all | solution.py:175
  115.1 78.2 %all-reduce.3.cloned.1.call-start = ((), (), s32[]{:S(2)}) async-start(), calls=%async_computation.7 | async-start | bytes 1048576 | tf_op jit(solution)/shard_map/psum | solution.py:182
  195.5 17.1 %all-to-all-start.1 = ((bf16[16,64,128]{2,1,0:T(8,128)(2,1)}), bf16[16,64,128]{2,1,0:T(8,128)(2,1)S(1)}, u32[]{:S(2)}, u32[]{:S(2)}) async-start(bf16[16,64,128]{2,1,0:T(8,128)(2,1)} %bitcast.78), calls=%async_computation.3 | async-start | bytes 524288 | tf_op jit(solution)/shard_map/all_to_all | solution.py:187
  (22 other events, 124.0 us)
Sparse Core Ops, SparseCore 0:
  37.6 10.4 reduce-scatter.2
  97.6 7.5 reduce-scatter.4
  108.6 62.7 all-gather.1
  175.9 17.3 all-reduce.2
